TPU v7x, 32 devices: a whole 2x2x4 slice. The times are simulated.
32 devices in a mesh: ep: 8 (over z, x), tp: 4 (over y, core).
Axes of the slice: x: 2, y: 2, z: 4, core: 2. Of those that a mesh axis runs over, the one named last changes fastest.
Arguments:
- residual_in: bfloat16 [128, 2048], P('ep'), may hold values from -6 to 6
- lengths: int32 [128], P('ep'), may hold values from 1 to 511, as said below
- kv_cache: bfloat16 [128, 4, 512, 256], P('ep', 'tp'), may hold values from -640 to 640
- norm_gain_attn: float32 [2048], replicated, may hold values from 0.1 to 1.9
- query_weight: bfloat16 [2048, 2048], P(None, 'tp'), may hold values from -0.125 to 0.125
- key_weight: bfloat16 [2048, 512], P(None, 'tp'), may hold values from -0.125 to 0.125
- value_weight: bfloat16 [2048, 512], P(None, 'tp'), may hold values from -0.125 to 0.125
- diff_lambda: float32 [16], P('tp'), may hold values from 0.3 to 0.8
- head_gain: float32 [128], replicated, may hold values from 0.1 to 1.9
- out_weight: bfloat16 [2048, 2048], P(None, 'tp'), may hold values from -0.125 to 0.125
- norm_gain_ffn: float32 [2048], replicated, may hold values from 0.1 to 1.9
- route_ids: int32 [128, 2], P('ep'), may hold values from 0 to 7, as said below
- route_weights: float32 [128, 2], P('ep'), may hold values from 0.1 to 1
- expert_gate: bfloat16 [8, 2048, 512], P('ep', None, 'tp'), may hold values from -0.125 to 0.125
- expert_up: bfloat16 [8, 2048, 512], P('ep', None, 'tp'), may hold values from -0.125 to 0.125
- expert_down: bfloat16 [8, 512, 2048], P('ep', 'tp'), may hold values from -0.25 to 0.25
- dense_gate: bfloat16 [2048, 8192], P(None, 'ep'), may hold values from -0.125 to 0.125
- dense_up: bfloat16 [2048, 8192], P(None, 'ep'), may hold values from -0.125 to 0.125
- dense_down: bfloat16 [8192, 2048], P('ep'), may hold values from -0.0625 to 0.0625
- dense_mix: float32 [2048], replicated, may hold values from -0.125 to 0.125
Outputs:
- layer_out: bfloat16 [128, 2048], P('ep', 'tp')
- new_rows: bfloat16 [128, 4, 256], P('ep', 'tp')
Inputs may be any that keep to these rules, and one draw needn't show every extreme that they name: The new token stands at position lengths[b]; some sequence holds 511 positions in every draw. `route_ids`: each row names 2 different experts from one group; the groups are the 4 runs of consecutive expert numbers of equal size. Among the rows of one index of ep no expert is named more than 8 times, and some expert exactly 8 times.
All inputs are finite; a program needn't handle non-finite values.
Results may differ from a plain program's by a relative error of at most 0.008.
The roundings to bfloat16 on the way count: a program that leaves them out, or rounds other values in their place, can miss the bound.
Values may be sent and summed in bfloat16 or wider, within the bound.
A program may use at most 64 MiB of HBM per device.

v0:
```python
import jax
import jax.numpy as jnp
from jax import lax
from jax.sharding import PartitionSpec as P

QK_DIM = 64
HEAD_DIM = 128
TOPK = 2


EPS = 1e-06


def rms_rows(values, gain):
    mean_sq = jnp.mean(values * values, axis=-1, keepdims=True)
    return values * lax.rsqrt(mean_sq + EPS) * gain


def rotate(vectors, positions):
    half = vectors.shape[-1] // 2
    inverse = 10000.0 ** (-jnp.arange(half, dtype=jnp.float32) / half)
    angle = positions[:, None, None, None] * inverse
    cosine = jnp.cos(angle)
    sine = jnp.sin(angle)
    first = vectors[..., :half]
    second = vectors[..., half:]
    return jnp.concatenate(
        [first * cosine - second * sine, first * sine + second * cosine], axis=-1
    )


def normalize(scores, latest, valid):
    masked = jnp.where(valid, scores, -jnp.inf)
    top = jnp.maximum(jnp.max(masked, axis=-1), latest)
    raised = jnp.where(valid, jnp.exp(jnp.where(valid, scores, 0.0) - top[..., None]), 0.0)
    raised_new = jnp.exp(latest - top)
    total = jnp.sum(raised, axis=-1) + raised_new
    return (raised / total[..., None], raised_new / total)


def attend(query, fresh, cache, lengths, lam):
    count = fresh.shape[0]
    groups = fresh.shape[1]
    share = query.shape[1] // groups
    scale = QK_DIM ** (-0.5)
    grouped = query.reshape(count, groups, share, 2, QK_DIM)
    first = (
        jnp.einsum(
            "bgjd,bgkd->bgjk",
            grouped[:, :, :, 0],
            cache[..., :QK_DIM],
            preferred_element_type=jnp.float32,
        )
        * scale
    )
    second = (
        jnp.einsum(
            "bgjd,bgkd->bgjk",
            grouped[:, :, :, 1],
            cache[..., QK_DIM : 2 * QK_DIM],
            preferred_element_type=jnp.float32,
        )
        * scale
    )
    first_new = (
        jnp.einsum(
            "bgjd,bgd->bgj",
            grouped[:, :, :, 0],
            fresh[..., :QK_DIM],
            preferred_element_type=jnp.float32,
        )
        * scale
    )
    second_new = (
        jnp.einsum(
            "bgjd,bgd->bgj",
            grouped[:, :, :, 1],
            fresh[..., QK_DIM : 2 * QK_DIM],
            preferred_element_type=jnp.float32,
        )
        * scale
    )
    valid = (
        jnp.arange(cache.shape[2], dtype=jnp.int32)[None, None, None, :]
        < lengths[:, None, None, None]
    )
    prob_one, prob_one_new = normalize(first, first_new, valid)
    prob_two, prob_two_new = normalize(second, second_new, valid)
    weight = lam.reshape(groups, share)[None, :, :, None]
    mapped = (prob_one - weight * prob_two).astype(jnp.bfloat16)
    mapped_new = (prob_one_new - weight[..., 0] * prob_two_new).astype(jnp.bfloat16)
    output = jnp.einsum(
        "bgjk,bgkd->bgjd", mapped, cache[..., 2 * QK_DIM :], preferred_element_type=jnp.float32
    )
    output = output + mapped_new.astype(jnp.float32)[..., None] * fresh[
        :, :, None, 2 * QK_DIM :
    ].astype(jnp.float32)
    return output.reshape(count, groups * share, HEAD_DIM)


def on_device(
    residual_in,
    lengths,
    kv_cache,
    norm_gain_attn,
    query_weight,
    key_weight,
    value_weight,
    diff_lambda,
    head_gain,
    out_weight,
    norm_gain_ffn,
    route_ids,
    route_weights,
    expert_gate,
    expert_up,
    expert_down,
    dense_gate,
    dense_up,
    dense_down,
    dense_mix,
):
    seq_count, width = residual_in.shape
    lanes = lax.axis_size("tp")
    column = lax.axis_index("tp")
    quarter = width // lanes
    groups = kv_cache.shape[1]
    local_heads = diff_lambda.shape[0]
    resid = residual_in.astype(jnp.float32)
    normed = rms_rows(resid, norm_gain_attn).astype(jnp.bfloat16)
    positions = lengths.astype(jnp.float32)
    query = jnp.dot(normed, query_weight, preferred_element_type=jnp.float32).reshape(
        seq_count, local_heads, 2, QK_DIM
    )
    query = rotate(query, positions).astype(jnp.bfloat16)
    keys = jnp.dot(normed, key_weight, preferred_element_type=jnp.float32).reshape(
        seq_count, groups, 2, QK_DIM
    )
    keys = rotate(keys, positions).astype(jnp.bfloat16).reshape(seq_count, groups, 2 * QK_DIM)
    values = (
        jnp.dot(normed, value_weight, preferred_element_type=jnp.float32)
        .reshape(seq_count, groups, HEAD_DIM)
        .astype(jnp.bfloat16)
    )
    fresh = jnp.concatenate([keys, values], axis=-1)
    mixed = attend(query, fresh, kv_cache, lengths, diff_lambda)
    heads_out = (
        rms_rows(mixed, head_gain).astype(jnp.bfloat16).reshape(seq_count, local_heads * HEAD_DIM)
    )
    all_heads = lax.all_gather(heads_out, "tp", axis=1, tiled=True)
    attn_cols = jnp.dot(all_heads, out_weight, preferred_element_type=jnp.float32)
    own_cols = lax.dynamic_slice_in_dim(resid, column * quarter, quarter, 1)
    stream_cols = (own_cols + attn_cols).astype(jnp.bfloat16)
    stream = lax.all_gather(stream_cols, "tp", axis=1, tiled=True)
    ffn_in = rms_rows(stream.astype(jnp.float32), norm_gain_ffn).astype(jnp.bfloat16)
    held = expert_gate.shape[0]
    expert_total = lax.axis_size("ep") * held
    capacity = max(2, 2 * TOPK * seq_count // expert_total)
    flat_ids = route_ids.reshape(-1)
    member = (flat_ids[:, None] == jnp.arange(expert_total, dtype=jnp.int32)[None, :]).astype(
        jnp.int32
    )
    slot = jnp.sum((jnp.cumsum(member, axis=0) - member) * member, axis=1)
    target = (flat_ids * capacity + slot).reshape(seq_count, TOPK)
    picker = (
        target[None, :, :] == jnp.arange(expert_total * capacity, dtype=jnp.int32)[:, None, None]
    )
    picker = jnp.any(picker, axis=2).astype(jnp.bfloat16)
    outgoing = jnp.dot(picker, ffn_in, preferred_element_type=jnp.float32).astype(jnp.bfloat16)
    outgoing = outgoing.reshape(expert_total, capacity, ffn_in.shape[1])
    arrived = lax.all_to_all(outgoing, "ep", split_axis=0, concat_axis=0, tiled=True)
    senders = arrived.shape[0] // held
    blocked = arrived.reshape(senders, held, arrived.shape[1], width)
    gate = jnp.einsum("sjcd,jdf->sjcf", blocked, expert_gate, preferred_element_type=jnp.float32)
    upward = jnp.einsum("sjcd,jdf->sjcf", blocked, expert_up, preferred_element_type=jnp.float32)
    hidden = (jax.nn.silu(gate) * upward).astype(jnp.bfloat16)
    partial_out = jnp.einsum(
        "sjcf,jfd->sjcd", hidden, expert_down, preferred_element_type=jnp.float32
    )
    partial_out = partial_out.reshape(arrived.shape[0], arrived.shape[1], width)
    summed = lax.psum_scatter(
        partial_out.astype(jnp.bfloat16), "tp", scatter_dimension=2, tiled=True
    )
    returned = lax.all_to_all(summed, "ep", split_axis=0, concat_axis=0, tiled=True)
    flat_back = returned.reshape(expert_total * capacity, quarter)
    picked = flat_back[target]
    expert_cols = jnp.sum(route_weights[..., None] * picked.astype(jnp.float32), axis=1)
    gate_mix = jax.nn.sigmoid(jnp.sum(ffn_in.astype(jnp.float32) * dense_mix, axis=-1))
    share_rows = seq_count // lanes
    mine = lax.dynamic_slice_in_dim(ffn_in, column * share_rows, share_rows, 0)
    piece = lax.all_gather(mine, "ep", axis=0, tiled=True)
    gate = jnp.dot(piece, dense_gate, preferred_element_type=jnp.float32)
    upward = jnp.dot(piece, dense_up, preferred_element_type=jnp.float32)
    dense_hidden = (jax.nn.silu(gate) * upward).astype(jnp.bfloat16)
    dense_cols = lax.psum_scatter(
        jnp.dot(dense_hidden, dense_down, preferred_element_type=jnp.float32),
        "ep",
        scatter_dimension=0,
        tiled=True,
    )
    dense_cols = lax.all_to_all(
        dense_cols.astype(jnp.bfloat16), "tp", split_axis=1, concat_axis=0, tiled=True
    ).astype(dense_cols.dtype)
    layer_out = (
        stream_cols.astype(jnp.float32) + expert_cols + gate_mix[:, None] * dense_cols
    ).astype(jnp.bfloat16)
    return (layer_out, fresh)


def solution(mesh):
    placed = (
        P("ep", None),
        P("ep"),
        P("ep", "tp", None, None),
        P(),
        P(None, "tp"),
        P(None, "tp"),
        P(None, "tp"),
        P("tp"),
        P(),
        P(None, "tp"),
        P(),
        P("ep", None),
        P("ep", None),
        P("ep", None, "tp"),
        P("ep", None, "tp"),
        P("ep", "tp", None),
        P(None, "ep"),
        P(None, "ep"),
        P("ep", None),
        P(),
    )
    return jax.shard_map(
        on_device,
        mesh=mesh,
        in_specs=placed,
        out_specs=(P("ep", "tp"), P("ep", "tp", None)),
        check_vma=False,
    )
```

profile of v0, /device:TPU:0, one launch (start us, length us, event | category | flops | bytes accessed | tf_op | source)
XLA Modules:
  0.0 165.9 jit_solution(6346756929134641032)
XLA Ops:
  7.2 0.0 copy-start
  7.2 0.8 convert_element_type.109
  8.0 0.7 iota_compare_fusion
  8.7 1.0 multiply_reduce_fusion.1
  9.7 0.9 convert_element_type.107
  10.6 1.3 fusion.73
  11.9 1.3 fusion.70
  13.2 0.1 reshape.337
  13.3 0.1 fusion.72
  13.5 1.3 fusion.69
  14.8 0.1 reshape.340
  14.9 0.1 multiply_cosine_fusion
  15.0 0.1 subtract_convert_fusion.1
  15.1 0.1 pad_maximum_fusion.1
  15.2 0.1 convert_element_type.110
  15.3 0.1 slice_bitcast_fusion.4
  15.4 0.1 fusion.55
  15.5 0.1 fusion.59
  15.6 2.5 %fusion.11 = f32[16,4,512]{2,1,0:T(4,128)S(1)} fusion(bf16[16,4,64]{2,1,0:T(4,128)(2,1)S(1)} %get-tuple-element.12, bf16[16,1,512,256]{3,2,1,0:T(8,128)(2,1)} %param.22), kind=kOutput, calls=%fused_computation.14 | convolution fusion | flops 4227072 | bytes 2236416 | tf_op jit(solution)/shard_map/bgjd,bgkd->bgjk/dot_general | solution.py:57
  18.2 0.1 fusion.61
  18.3 2.3 %select_reduce_fusion.1 = (f32[16,4]{1,0:T(8,128)S(1)}, f32[16,4]{1,0:T(8,128)S(1)}, f32[16,4,512]{2,1,0:T(4,128)S(1)}) fusion(pred[16,512]{1,0:T(8,128)(4,1)S(1)} %iota_compare_fusion, f32[16,4,512]{2,1,0:T(4,128)S(1)} %fusion.11, bf16[16,4,64]{2,1,0:T(4,128)(2,1)S(1)} %get-tuple-element.13, bf16[16,1,512,256]{3,2,1,0:T(8,128)(2,1)} %param.22), kind=kOutput, calls=%fused_computation.44 | convolution fusion | flops 4358016 | bytes 2376192 | tf_op jit(solution)/shard_map/bgjd,bgkd->bgjk/dot_general | solution.py:48
  20.6 0.0 copy-start.4
  20.7 0.3 fusion.34
  21.0 0.6 multiply_reduce_fusion.3
  21.6 0.1 broadcast_multiply_fusion
  21.7 6.2 %all_gather.9 = bf16[16,2048]{1,0:T(8,128)(2,1)S(1)} all-gather(bf16[16,512]{1,0:T(8,128)(2,1)S(1)} %fusion.45), channel_id=1, replica_groups=mesh['ep'=8,'tp'=4] {'tp'}, dimensions={1}, use_global_device_ids=true | all-gather | bytes 81920 | tf_op jit(solution)/shard_map/all_gather | solution.py:150
  28.0 2.0 %fusion.18 = bf16[16,512]{1,0:T(8,128)(2,1)S(1)} fusion(bf16[16,2048]{1,0:T(8,128)(2,1)S(1)} %all_gather.9, bf16[2048,512]{1,0:T(8,128)(2,1)} %param.29, f32[16,2048]{1,0:T(8,128)S(1)} %convert_element_type.107, s32[]{:T(128)S(6)} %select_n.34), kind=kOutput, calls=%fused_computation.22 | convolution fusion | flops 33570816 | bytes 2211844 | tf_op jit(solution)/shard_map/dot_general | solution.py:151
  29.9 5.5 %all_gather.10 = bf16[16,2048]{1,0:T(8,128)(2,1)S(1)} all-gather(bf16[16,512]{1,0:T(8,128)(2,1)S(1)} %fusion.18), channel_id=1, replica_groups=mesh['ep'=8,'tp'=4] {'tp'}, dimensions={1}, use_global_device_ids=true | all-gather | bytes 81920 | tf_op jit(solution)/shard_map/all_gather | solution.py:154
  35.5 0.1 fusion.25
  35.6 0.1 copy.69
  35.7 0.1 eq.28
  35.8 0.1 fusion.57
  35.9 0.1 reduce_window_sum.11
  35.9 0.2 select_reduce_fusion.2
  36.1 0.1 reduce_sum.79
  36.2 0.1 copy.70
  36.3 0.1 fusion.58
  36.4 0.0 copy-done.4
  36.4 0.2 multiply_reduce_fusion
  36.6 1.0 fusion
  37.6 6.0 %all-to-all-start = ((bf16[8,8,2048]{2,1,0:T(8,128)(2,1)}), bf16[8,8,2048]{2,1,0:T(8,128)(2,1)S(1)}, u32[]{:S(2)}, u32[]{:S(2)}) async-start(bf16[8,8,2048]{2,1,0:T(8,128)(2,1)} %fusion), calls=%async_computation | async-start | bytes 524288 | tf_op jit(solution)/shard_map/all_to_all | solution.py:171
  43.5 0.0 reduce-scatter.2.cloned.1.call-start
  43.6 33.4 %all-gather = bf16[8,4,2048]{2,1,0:T(4,128)(2,1)S(1)} all-gather(bf16[1,4,2048]{2,1,0:T(4,128)(2,1)S(1)} %dynamic-slice_bitcast_fusion), channel_id=1, replica_groups=mesh['ep'=8,'tp'=4] {'ep'}, dimensions={0}, use_global_device_ids=true | all-gather | bytes 147456 | tf_op jit(solution)/shard_map/all_gather | solution.py:191
  77.1 3.0 %fusion.74 = f32[32,1024]{1,0:T(8,128)S(1)} fusion(bf16[32,2048]{1,0:T(8,128)(2,1)S(1)} %reshape.365, bf16[2048,1024]{1,0:T(8,128)(2,1)} %param.36), kind=kOutput, calls=%fused_computation.125 | convolution fusion | flops 134217728 | bytes 4456448 | tf_op jit(solution)/shard_map/dot_general | solution.py:192
  80.1 0.0 copy-start.2
  80.1 5.1 %fusion.15 = f32[32,2048]{1,0:T(8,128)S(1)} fusion(bf16[1024,2048]{1,0:T(8,128)(2,1)} %param.38, bf16[32,2048]{1,0:T(8,128)(2,1)S(1)} %reshape.365, bf16[2048,1024]{1,0:T(8,128)(2,1)} %param.37, f32[32,1024]{1,0:T(8,128)S(1)} %fusion.74), kind=kOutput, calls=%fused_computation.16 | convolution fusion | flops 268632064 | bytes 8912896 | tf_op jit(solution)/shard_map/dot_general | solution.py:196
  85.2 0.6 dynamic-slice
  86.4 37.8 %all-reduce.2 = bf16[32,2048]{1,0:T(8,128)(2,1)S(1)} all-reduce(f32[32,2048]{1,0:T(8,128)S(1)} %fusion.15), channel_id=3, replica_groups=mesh['ep'=8,'tp'=4] {'ep'}, use_global_device_ids=true, to_apply=%region_13.14.clone | all-reduce | flops 65536 | bytes 393216
  124.2 1.3 convolution_bitcast_fusion.1
  125.5 2.1 %convolution_convert_fusion = bf16[8,8,2048]{2,1,0:T(8,128)(2,1)} fusion(bf16[8,8,2048]{2,1,0:T(8,128)(2,1)S(1)} %all-to-all-done, bf16[1,128,2048]{2,1,0:T(8,128)(2,1)S(1)} %copy-done.2, bf16[1,2048,128]{2,1,0:T(8,128)(2,1)} %param.34, f32[8,1,8,128]{3,2,0,1:T(8,128)S(1)} %convolution_bitcast_fusion.1), kind=kOutput, calls=%fused_computation.1 | convolution fusion | flops 67289088 | bytes 1605632 | tf_op jit(solution)/shard_map/sjcf,jfd->sjcd/dot_general | solution.py:177
  127.6 0.0 reduce-scatter.2.cloned.1.call-update
  127.6 0.6 dynamic-slice_convert_fusion
  128.3 3.3 %all-to-all-start.2 = ((bf16[4,4,512]{2,0,1:T(4,128)(2,1)}), bf16[4,4,512]{2,0,1:T(4,128)(2,1)S(1)}, u32[]{:S(2)}, u32[]{:S(2)}) async-start(bf16[4,4,512]{2,0,1:T(4,128)(2,1)} %bitcast.35), calls=%async_computation.3 | async-start | bytes 32768 | tf_op jit(solution)/shard_map/all_to_all | solution.py:201
  131.5 0.1 copy.71
  131.6 0.1 reshape.355
  131.7 0.6 pad_maximum_fusion.2
  132.3 0.1 copy.68
  132.4 2.9 %all-to-all-done.2 = bf16[4,4,512]{2,0,1:T(4,128)(2,1)S(1)} async-done(((bf16[4,4,512]{2,0,1:T(4,128)(2,1)}), bf16[4,4,512]{2,0,1:T(4,128)(2,1)S(1)}, u32[]{:S(2)}, u32[]{:S(2)}) %all-to-all-start.2) | async-done | bytes 16416 | tf_op jit(solution)/shard_map/all_to_all | solution.py:201
  135.4 9.8 %reduce-scatter.2.cloned.1.call-done = bf16[8,8,512]{2,1,0:T(8,128)(2,1)} async-done(((bf16[8,8,2048]{2,1,0:T(8,128)(2,1)}), bf16[8,8,512]{2,1,0:T(8,128)(2,1)}) %reduce-scatter.2.cloned.1.call-update) | async-done | bytes 65552 | tf_op jit(solution)/shard_map/reduce_scatter | solution.py:181
  145.2 5.5 %all-to-all-start.1 = ((bf16[8,8,512]{2,1,0:T(8,128)(2,1)}), bf16[8,8,512]{2,1,0:T(8,128)(2,1)S(1)}, u32[]{:S(2)}, u32[]{:S(2)}) async-start(bf16[8,8,512]{2,1,0:T(8,128)(2,1)} %reduce-scatter.2.cloned.1.call-done), calls=%async_computation.2 | async-start | bytes 131072 | tf_op jit(solution)/shard_map/all_to_all | solution.py:184
  150.7 6.9 %all-to-all-done.1 = bf16[8,8,512]{2,1,0:T(8,128)(2,1)S(1)} async-done(((bf16[8,8,512]{2,1,0:T(8,128)(2,1)}), bf16[8,8,512]{2,1,0:T(8,128)(2,1)S(1)}, u32[]{:S(2)}, u32[]{:S(2)}) %all-to-all-start.1) | async-done | bytes 65568 | tf_op jit(solution)/shard_map/all_to_all | solution.py:184
  157.6 0.6 gather_fusion
  158.2 0.1 multiply_reduce_fusion.2
  158.4 0.7 add_convert_fusion.1
  (34 shorter events, 0.3 us)
Async XLA Ops:
  7.2 4.7 %copy-start = (bf16[2048,512]{1,0:T(8,128)(2,1)S(1)}, bf16[2048,512]{1,0:T(8,128)(2,1)}, u32[]{:S(2)}) copy-start(bf16[2048,512]{1,0:T(8,128)(2,1)} %param.24) | copy-start | bytes 6291460
  11.9 9.1 %copy-start.7 = (f32[4]{0:T(128)S(1)}, f32[4]{0:T(128)}, u32[]{:S(2)}) copy-start(f32[4]{0:T(128)} %param.27) | copy-start | bytes 52
  15.3 5.7 %copy-start.1 = (bf16[16,1,512,256]{3,2,1,0:T(8,128)(2,1)S(1)}, bf16[16,1,512,256]{3,2,1,0:T(8,128)(2,1)}, u32[]{:S(2)}) copy-start(bf16[16,1,512,256]{3,2,1,0:T(8,128)(2,1)} %param.22) | copy-start | bytes 12582916
  18.2 3.5 %copy-start.8 = (f32[128]{0:T(128)S(1)}, f32[128]{0:T(128)}, u32[]{:S(2)}) copy-start(f32[128]{0:T(128)} %param.28) | copy-start | bytes 1540
  20.6 15.0 %copy-start.5 = (s32[16,2]{0,1:T(2,128)S(1)}, s32[16,2]{0,1:T(2,128)}, u32[]{:S(2)}) copy-start(s32[16,2]{0,1:T(2,128)} %param.31) | copy-start | bytes 388
  20.6 15.7 %copy-start.3 = (f32[2048]{0:T(1024)S(1)}, f32[2048]{0:T(1024)}, u32[]{:S(2)}) copy-start(f32[2048]{0:T(1024)} %param.39) | copy-start | bytes 24580
  20.6 15.7 %copy-start.4 = (f32[2048]{0:T(1024)S(1)}, f32[2048]{0:T(1024)}, u32[]{:S(2)}) copy-start(f32[2048]{0:T(1024)} %param.30) | copy-start | bytes 24580
  37.6 86.6 %all-to-all-start = ((bf16[8,8,2048]{2,1,0:T(8,128)(2,1)}), bf16[8,8,2048]{2,1,0:T(8,128)(2,1)S(1)}, u32[]{:S(2)}, u32[]{:S(2)}) async-start(bf16[8,8,2048]{2,1,0:T(8,128)(2,1)} %fusion), calls=%async_computation | async-start | bytes 524288 | tf_op jit(solution)/shard_map/all_to_all | solution.py:171
  43.5 101.6 %reduce-scatter.2.cloned.1.call-start = ((), (), s32[]{:S(2)}) async-start(), calls=%async_computation.4 | async-start | bytes 327680 | tf_op jit(solution)/shard_map/reduce_scatter | solution.py:181
  80.1 5.1 %copy-start.9 = (u32[32]{0:T(128)S(1)}, u32[32]{0:T(128)}, u32[]{:S(2)}) copy-start(u32[32]{0:T(128)} %constant.59) | copy-start | bytes 388
  80.1 45.4 %copy-start.2 = (bf16[1,128,2048]{2,1,0:T(8,128)(2,1)S(1)}, bf16[1,128,2048]{2,1,0:T(8,128)(2,1)}, u32[]{:S(2)}) copy-start(bf16[1,128,2048]{2,1,0:T(8,128)(2,1)} %param.35) | copy-start | bytes 1572868
  80.1 52.2 %copy-start.6 = (f32[16,2]{0,1:T(2,128)S(1)}, f32[16,2]{0,1:T(2,128)}, u32[]{:S(2)}) copy-start(f32[16,2]{0,1:T(2,128)} %param.32) | copy-start | bytes 388
  128.3 7.1 %all-to-all-start.2 = ((bf16[4,4,512]{2,0,1:T(4,128)(2,1)}), bf16[4,4,512]{2,0,1:T(4,128)(2,1)S(1)}, u32[]{:S(2)}, u32[]{:S(2)}) async-start(bf16[4,4,512]{2,0,1:T(4,128)(2,1)} %bitcast.35), calls=%async_computation.3 | async-start | bytes 32768 | tf_op jit(solution)/shard_map/all_to_all | solution.py:201
  145.2 12.4 %all-to-all-start.1 = ((bf16[8,8,512]{2,1,0:T(8,128)(2,1)}), bf16[8,8,512]{2,1,0:T(8,128)(2,1)S(1)}, u32[]{:S(2)}, u32[]{:S(2)}) async-start(bf16[8,8,512]{2,1,0:T(8,128)(2,1)} %reduce-scatter.2.cloned.1.call-done), calls=%async_computation.2 | async-start | bytes 131072 | tf_op jit(solution)/shard_map/all_to_all | solution.py:184
Sparse Core Ops, SparseCore 0:
  127.8 17.3 reduce-scatter.1
where the time goes:
time: 167 us; the launch traced here: 166 us
  blocking collectives  82.9 us (50%)
  matrix products  24.1 us (14%)
  waiting for transfers between devices  19.6 us (12%)
  between operations  15 us (9%)
  starting transfers between devices  14.8 us (9%)
  other arithmetic  6.43 us (4%)
  local copies, waits for them, and re-layouts  3.1 us (2%)
    unnamed x1, blocking collectives  37.8 us
    all_gather x1, blocking collectives, on_device(): piece = lax.all_gather(mine, 'ep', axis=0, tiled=True)  33.4 us
    reduce_scatter x1, waiting for transfers between devices, on_device(): lax.psum_scatter(partial_out.astype(jnp.bfloat16), 'tp', scatter_dimensio...  9.79 us
    all_to_all x1, waiting for transfers between devices, on_device(): lax.all_to_all(summed, 'ep', split_axis=0, concat_axis=0, tiled=True)  6.88 us
    all_gather x1, blocking collectives, on_device(): all_heads = lax.all_gather(heads_out, 'tp', axis=1, tiled=True)  6.24 us
    all_to_all x1, starting transfers between devices, on_device(): lax.all_to_all(outgoing, 'ep', split_axis=0, concat_axis=0, tiled=True)  5.98 us
    all_gather x1, blocking collectives, on_device(): stream = lax.all_gather(stream_cols, 'tp', axis=1, tiled=True)  5.52 us
    all_to_all x1, starting transfers between devices, on_device(): lax.all_to_all(summed, 'ep', split_axis=0, concat_axis=0, tiled=True)  5.5 us
  transfers between devices with their start and end apart: 4, of which 3 were waited for; matrix products, arithmetic and copies ran while one was open for 6% of the time, Pallas kernels for 0%

commit v1 on v0

--- a/solution.py
+++ b/solution.py
@@ -1,11 +1,14 @@
+import functools
+
 import jax
 import jax.numpy as jnp
 from jax import lax
+from jax.experimental import pallas as pl
+from jax.experimental.pallas import tpu as pltpu
 from jax.sharding import PartitionSpec as P
 
 QK_DIM = 64
 HEAD_DIM = 128
-TOPK = 2
 
 
 EPS = 1e-06
@@ -96,6 +99,447 @@
         :, :, None, 2 * QK_DIM :
     ].astype(jnp.float32)
     return output.reshape(count, groups * share, HEAD_DIM)
+
+
+MESH = pl.DeviceIdType.MESH
+F32 = jnp.float32
+BF16 = jnp.bfloat16
+LANES = 128
+
+
+def flip(value, mask):
+    bit = 1
+    while bit <= mask:
+        if mask & bit:
+            value = value + bit * (1 - 2 * ((value // bit) % 2))
+        bit *= 2
+    return value
+
+
+def each(count, body, order=None):
+    if count <= 16:
+        for index in order if order is not None else range(count):
+            body(index)
+    else:
+
+        def step(index, carry):
+            body(index)
+            return carry
+
+        lax.fori_loop(0, count, step, 0)
+
+
+def block(start, size):
+    return pl.ds(pl.multiple_of(start * size, size), size)
+
+
+def remote(source, target, send, recv, where):
+    return pltpu.make_async_remote_copy(
+        src_ref=source,
+        dst_ref=target,
+        send_sem=send,
+        recv_sem=recv,
+        device_id=where,
+        device_id_type=MESH,
+    )
+
+
+def dot(left, right):
+    return jnp.dot(left, right, preferred_element_type=F32)
+
+
+def layer_kernel(
+    n_ep,
+    n_tp,
+    split,
+    heads_ref,
+    resid_ref,
+    gain_ref,
+    mixw_ref,
+    ids_ref,
+    rw_ref,
+    ow_hbm,
+    eg_hbm,
+    eu_hbm,
+    ed_hbm,
+    dg_hbm,
+    du_hbm,
+    dd_hbm,
+    out_ref,
+    ow,
+    eg,
+    eu,
+    ed,
+    dg,
+    du,
+    dd,
+    heads_all,
+    stream,
+    ffn,
+    mix,
+    route,
+    eh,
+    dh,
+    away,
+    came,
+    summed,
+    landed,
+    w_sem,
+    route_send,
+    route_recv,
+    heads_send,
+    heads_recv,
+    first_send,
+    second_send,
+    relay_send,
+    stream_recv,
+    pair_send,
+    pair_recv,
+    back_send,
+    back_recv,
+):
+    e = lax.axis_index("ep")
+    t = lax.axis_index("tp")
+    half = n_tp // 2
+    mate = flip(t, 1)
+    core = t % 2
+    seqs, width = resid_ref.shape
+    quarter = out_ref.shape[1]
+    held, _, part = eg.shape
+    hid = dg.shape[1]
+    rows_all = n_ep * seqs
+    evens = [2 * i for i in range(1, half)]
+
+    barrier = pltpu.get_barrier_semaphore()
+
+    def greet(index):
+        where = (index // half, 2 * (index % half) + core)
+
+        @pl.when(jnp.logical_or(where[0] != e, where[1] != t))
+        def _():
+            pl.semaphore_signal(barrier, inc=1, device_id=where, device_id_type=MESH)
+
+    each(n_ep * half, greet)
+    for i in range(half):
+        pl.semaphore_signal(
+            barrier, inc=1, device_id=(e, 2 * i + 1 - core), device_id_type=MESH
+        )
+
+    if split:
+        cols = block(t, hid)
+        dense_parts = (dg_hbm.at[:, cols], du_hbm.at[:, cols], dd_hbm.at[cols, :])
+    else:
+        dense_parts = (dg_hbm, du_hbm, dd_hbm)
+    loads = [
+        pltpu.make_async_copy(src, dst, w_sem.at[i])
+        for i, (src, dst) in enumerate(
+            zip((ow_hbm, eg_hbm, eu_hbm) + dense_parts[:2] + (ed_hbm, dense_parts[2]), (ow, eg, eu, dg, du, ed, dd))
+        )
+    ]
+    for load in loads:
+        load.start()
+
+    lane = lax.broadcasted_iota(jnp.int32, (seqs, route.shape[1]), 1)
+    table = jnp.zeros((seqs, route.shape[1]), F32)
+    for k in range(ids_ref.shape[1]):
+        table = table + jnp.where(lane == ids_ref[:, k : k + 1], rw_ref[:, k : k + 1], 0.0)
+    own_rows = block(e, seqs)
+    route[own_rows, :] = table
+
+    pl.semaphore_wait(barrier, n_ep * half - 1 + half)
+
+    def heads_copy(mask):
+        return remote(
+            heads_ref,
+            heads_all.at[mask - 1],
+            heads_send.at[mask - 1],
+            heads_recv.at[mask - 1],
+            (e, flip(t, mask)),
+        )
+
+    for mask in range(n_tp - 1, 0, -1):
+        heads_copy(mask).start()
+
+    def route_copy(d):
+        there = (e + d) % n_ep
+        return remote(
+            route.at[own_rows, :],
+            route.at[own_rows, :],
+            route_send.at[d - 1],
+            route_recv.at[d - 1],
+            (there, t),
+        )
+
+    def route_wait(d):
+        came_from = (e + n_ep - d) % n_ep
+        spot = route.at[block(came_from, seqs), :]
+        remote(spot, spot, route_send.at[d - 1], route_recv.at[d - 1], (e, t)).wait_recv()
+
+    each(n_ep - 1, lambda i: route_copy(i + 1).start())
+
+    loads[0].wait()
+    span = heads_ref.shape[1]
+    total = dot(heads_ref[...], ow[block(t, span), :])
+    for mask in range(1, n_tp):
+        heads_copy(mask).wait_recv()
+        total = total + dot(heads_all[mask - 1], ow[block(flip(t, mask), span), :])
+    own_cols = block(t, quarter)
+    own_stream = (resid_ref[:, own_cols].astype(F32) + total).astype(BF16)
+    stream[own_rows, own_cols] = own_stream
+
+    def spot(owner, column):
+        return stream.at[block(owner, seqs), block(column, quarter)]
+
+    def owner_of(d):
+        return (e + n_ep - d) % n_ep
+
+    def first(d):
+        return remote(
+            spot(e, t), spot(e, t), first_send.at[d], stream_recv.at[0, d], ((e + d) % n_ep, t)
+        )
+
+    def second(d, mask):
+        index = mask // 2 if mask != 1 else 0
+        where = spot(owner_of(d), t)
+        return remote(
+            where, where, second_send.at[index, d], stream_recv.at[mask, d], (e, flip(t, mask))
+        )
+
+    def relay(d, mask):
+        where = spot(owner_of(d), flip(t, mask))
+        return remote(
+            where, where, relay_send.at[mask // 2 - 1, d], stream_recv.at[mask + 1, d], (e, mate)
+        )
+
+    def arrived(d, mask):
+        where = spot(owner_of(d), flip(t, mask))
+        remote(where, where, first_send.at[d], stream_recv.at[mask, d], (e, t)).wait_recv()
+
+    def spread(d):
+        for mask in evens:
+            second(d, mask).start()
+        second(d, 1).start()
+
+    far_first = sorted(range(1, n_ep), key=lambda d: -min(d, n_ep - d)) if n_ep <= 16 else None
+    near_first = [0] + far_first[::-1] if far_first is not None else None
+    each(n_ep - 1 if far_first is None else 1, lambda i: first(i + 1).start(), order=None) if far_first is None else [
+        first(d).start() for d in far_first
+    ]
+
+    def stage_two(d):
+        if not (isinstance(d, int) and d == 0):
+            arrived(d, 0)
+        spread(d)
+
+    def stage_three(d):
+        for mask in evens:
+            arrived(d, mask)
+            relay(d, mask).start()
+
+    def normalise(d):
+        arrived(d, 1)
+        for mask in evens:
+            arrived(d, mask + 1)
+        rows = block(owner_of(d), seqs)
+        values = stream[rows, :].astype(F32)
+        mean_sq = jnp.mean(values * values, axis=-1, keepdims=True)
+        scaled = (values * lax.rsqrt(mean_sq + EPS) * gain_ref[...]).astype(BF16)
+        ffn[rows, :] = scaled
+        inner = jnp.sum(scaled.astype(F32) * mixw_ref[...], axis=-1, keepdims=True)
+        mix[rows, :] = jnp.broadcast_to(jax.nn.sigmoid(inner), (seqs, LANES))
+
+    if near_first is not None:
+        for i, d in enumerate(near_first):
+            stage_two(d)
+            if i:
+                stage_three(near_first[i - 1])
+            if i > 1:
+                normalise(near_first[i - 2])
+        stage_three(near_first[-1])
+        for d in near_first[-2:]:
+            normalise(d)
+    else:
+        stage_two(0)
+        each(n_ep - 1, lambda i: stage_two(i + 1))
+        each(n_ep, stage_three)
+        each(n_ep, normalise)
+    each(n_ep - 1, lambda i: route_wait(i + 1))
+
+    many = min(rows_all, 128)
+    batches = rows_all // many
+    for load in loads[1:5]:
+        load.wait()
+
+    def hidden(b):
+        rows = block(b, many)
+        a = ffn[rows, :]
+        for j in range(held):
+            eh[j, rows, :] = (jax.nn.silu(dot(a, eg[j])) * dot(a, eu[j])).astype(BF16)
+        units = jax.nn.silu(dot(a, dg[...])) * dot(a, du[...])
+        if not split:
+            own = hid // n_tp
+            unit = lax.broadcasted_iota(jnp.int32, units.shape, 1)
+            units = jnp.where((unit >= t * own) & (unit < (t + 1) * own), units, 0.0)
+        dh[rows, :] = units.astype(BF16)
+
+    each(batches, hidden)
+    for load in loads[5:]:
+        load.wait()
+
+    def result(b, q):
+        rows = block(b, many)
+        cols = block(q, quarter)
+        total = mix[rows, :1] * dot(dh[rows, :], dd[:, cols])
+        lanes = lax.broadcasted_iota(jnp.int32, (many, route.shape[1]), 1)
+        for j in range(held):
+            weight = jnp.sum(
+                jnp.where(lanes == e * held + j, route[rows, :], 0.0), axis=1, keepdims=True
+            )
+            piece = dot(eh[j, rows, :], ed[j, :, cols]).astype(BF16)
+            total = total + weight * piece.astype(F32)
+        return total
+
+    def pair(j):
+        return remote(away.at[j], came.at[j], pair_send.at[j], pair_recv.at[j], (e, mate))
+
+    for j in range(half):
+
+        def leave(b, j=j):
+            away[j, block(b, many), :] = result(b, 2 * j + 1 - core).astype(BF16)
+
+        each(batches, leave)
+        pair(j).start()
+
+    me = e * half + t // 2
+
+    def back(j, d):
+        there = (e + d) % n_ep
+        return remote(
+            summed.at[j, block(there, seqs), :],
+            landed.at[me],
+            back_send.at[j, d],
+            back_recv.at[me],
+            (there, 2 * j + core),
+        )
+
+    def same(j, d):
+        return jnp.logical_and(jnp.asarray(d == 0), 2 * j + core == t)
+
+    for j in range(half):
+
+        def keep(b, j=j):
+            summed[j, block(b, many), :] = result(b, 2 * j + core).astype(BF16)
+
+        each(batches, keep)
+    for j in range(half):
+        pair(j).wait_recv()
+
+        def add(b, j=j):
+            rows = block(b, many)
+            summed[j, rows, :] = (summed[j, rows, :].astype(F32) + came[j, rows, :].astype(F32)).astype(BF16)
+
+        each(batches, add)
+
+        def send(d, j=j):
+            @pl.when(jnp.logical_not(same(j, d)))
+            def _():
+                back(j, d).start()
+
+        each(n_ep, send, order=None if far_first is None else far_first + [0])
+
+    landed[me] = summed[t // 2, own_rows, :]
+
+    def take(index):
+        @pl.when(index != me)
+        def _():
+            where = landed.at[index]
+            remote(where, where, back_send.at[0, 0], back_recv.at[index], (e, t)).wait_recv()
+
+    each(n_ep * half, take)
+    out_ref[...] = (
+        own_stream.astype(F32) + jnp.sum(landed[...].astype(F32), axis=0)
+    ).astype(BF16)
+
+    for mask in range(1, n_tp):
+        heads_copy(mask).wait_send()
+    each(n_ep - 1, lambda i: route_copy(i + 1).wait_send())
+    each(n_ep - 1, lambda i: first(i + 1).wait_send())
+
+    def sent(d):
+        second(d, 1).wait_send()
+        for mask in evens:
+            second(d, mask).wait_send()
+            relay(d, mask).wait_send()
+
+    each(n_ep, sent)
+    for j in range(half):
+        pair(j).wait_send()
+
+        def gone(d, j=j):
+            @pl.when(jnp.logical_not(same(j, d)))
+            def _():
+                back(j, d).wait_send()
+
+        each(n_ep, gone)
+
+
+def layer_call(heads, resid, gain, mixw, ids, rw, ow, eg, eu, ed, dg, du, dd):
+    n_ep = lax.axis_size("ep")
+    n_tp = lax.axis_size("tp")
+    half = n_tp // 2
+    seqs, width = resid.shape
+    quarter = ow.shape[1]
+    held, _, part = eg.shape
+    rows = n_ep * seqs
+    own = dg.shape[1] // n_tp
+    split = own % LANES == 0
+    hid = own if split else dg.shape[1]
+    lanes = -(-n_ep * held // LANES) * LANES
+    vmem = pl.BlockSpec(memory_space=pltpu.VMEM)
+    hbm = pl.BlockSpec(memory_space=pl.ANY)
+    dma = pltpu.SemaphoreType.DMA
+    return pl.pallas_call(
+        functools.partial(layer_kernel, n_ep, n_tp, split),
+        out_shape=jax.ShapeDtypeStruct((seqs, quarter), BF16),
+        in_specs=[vmem] * 6 + [hbm] * 7,
+        out_specs=vmem,
+        scratch_shapes=[
+            pltpu.VMEM(ow.shape, BF16),
+            pltpu.VMEM(eg.shape, BF16),
+            pltpu.VMEM(eu.shape, BF16),
+            pltpu.VMEM(ed.shape, BF16),
+            pltpu.VMEM((width, hid), BF16),
+            pltpu.VMEM((width, hid), BF16),
+            pltpu.VMEM((hid, width), BF16),
+            pltpu.VMEM((n_tp - 1,) + heads.shape, BF16),
+            pltpu.VMEM((rows, width), BF16),
+            pltpu.VMEM((rows, width), BF16),
+            pltpu.VMEM((rows, LANES), F32),
+            pltpu.VMEM((rows, lanes), F32),
+            pltpu.VMEM((held, rows, part), BF16),
+            pltpu.VMEM((rows, hid), BF16),
+            pltpu.VMEM((half, rows, quarter), BF16),
+            pltpu.VMEM((half, rows, quarter), BF16),
+            pltpu.VMEM((half, rows, quarter), BF16),
+            pltpu.VMEM((n_ep * half, seqs, quarter), BF16),
+            dma((7,)),
+            dma((n_ep - 1,)),
+            dma((n_ep - 1,)),
+            dma((n_tp - 1,)),
+            dma((n_tp - 1,)),
+            dma((n_ep,)),
+            dma((half, n_ep)),
+            dma((max(half - 1, 1), n_ep)),
+            dma((n_tp, n_ep)),
+            dma((half,)),
+            dma((half,)),
+            dma((half, n_ep)),
+            dma((n_ep * half,)),
+        ],
+        compiler_params=pltpu.CompilerParams(
+            collective_id=0, has_side_effects=True, vmem_limit_bytes=56 * 1024 * 1024
+        ),
+    )(heads, resid, gain, mixw, ids, rw, ow, eg, eu, ed, dg, du, dd)
 
 
 def on_device(
@@ -121,9 +565,6 @@
     dense_mix,
 ):
     seq_count, width = residual_in.shape
-    lanes = lax.axis_size("tp")
-    column = lax.axis_index("tp")
-    quarter = width // lanes
     groups = kv_cache.shape[1]
     local_heads = diff_lambda.shape[0]
     resid = residual_in.astype(jnp.float32)
@@ -147,63 +588,21 @@
     heads_out = (
         rms_rows(mixed, head_gain).astype(jnp.bfloat16).reshape(seq_count, local_heads * HEAD_DIM)
     )
-    all_heads = lax.all_gather(heads_out, "tp", axis=1, tiled=True)
-    attn_cols = jnp.dot(all_heads, out_weight, preferred_element_type=jnp.float32)
-    own_cols = lax.dynamic_slice_in_dim(resid, column * quarter, quarter, 1)
-    stream_cols = (own_cols + attn_cols).astype(jnp.bfloat16)
-    stream = lax.all_gather(stream_cols, "tp", axis=1, tiled=True)
-    ffn_in = rms_rows(stream.astype(jnp.float32), norm_gain_ffn).astype(jnp.bfloat16)
-    held = expert_gate.shape[0]
-    expert_total = lax.axis_size("ep") * held
-    capacity = max(2, 2 * TOPK * seq_count // expert_total)
-    flat_ids = route_ids.reshape(-1)
-    member = (flat_ids[:, None] == jnp.arange(expert_total, dtype=jnp.int32)[None, :]).astype(
-        jnp.int32
-    )
-    slot = jnp.sum((jnp.cumsum(member, axis=0) - member) * member, axis=1)
-    target = (flat_ids * capacity + slot).reshape(seq_count, TOPK)
-    picker = (
-        target[None, :, :] == jnp.arange(expert_total * capacity, dtype=jnp.int32)[:, None, None]
-    )
-    picker = jnp.any(picker, axis=2).astype(jnp.bfloat16)
-    outgoing = jnp.dot(picker, ffn_in, preferred_element_type=jnp.float32).astype(jnp.bfloat16)
-    outgoing = outgoing.reshape(expert_total, capacity, ffn_in.shape[1])
-    arrived = lax.all_to_all(outgoing, "ep", split_axis=0, concat_axis=0, tiled=True)
-    senders = arrived.shape[0] // held
-    blocked = arrived.reshape(senders, held, arrived.shape[1], width)
-    gate = jnp.einsum("sjcd,jdf->sjcf", blocked, expert_gate, preferred_element_type=jnp.float32)
-    upward = jnp.einsum("sjcd,jdf->sjcf", blocked, expert_up, preferred_element_type=jnp.float32)
-    hidden = (jax.nn.silu(gate) * upward).astype(jnp.bfloat16)
-    partial_out = jnp.einsum(
-        "sjcf,jfd->sjcd", hidden, expert_down, preferred_element_type=jnp.float32
-    )
-    partial_out = partial_out.reshape(arrived.shape[0], arrived.shape[1], width)
-    summed = lax.psum_scatter(
-        partial_out.astype(jnp.bfloat16), "tp", scatter_dimension=2, tiled=True
-    )
-    returned = lax.all_to_all(summed, "ep", split_axis=0, concat_axis=0, tiled=True)
-    flat_back = returned.reshape(expert_total * capacity, quarter)
-    picked = flat_back[target]
-    expert_cols = jnp.sum(route_weights[..., None] * picked.astype(jnp.float32), axis=1)
-    gate_mix = jax.nn.sigmoid(jnp.sum(ffn_in.astype(jnp.float32) * dense_mix, axis=-1))
-    share_rows = seq_count // lanes
-    mine = lax.dynamic_slice_in_dim(ffn_in, column * share_rows, share_rows, 0)
-    piece = lax.all_gather(mine, "ep", axis=0, tiled=True)
-    gate = jnp.dot(piece, dense_gate, preferred_element_type=jnp.float32)
-    upward = jnp.dot(piece, dense_up, preferred_element_type=jnp.float32)
-    dense_hidden = (jax.nn.silu(gate) * upward).astype(jnp.bfloat16)
-    dense_cols = lax.psum_scatter(
-        jnp.dot(dense_hidden, dense_down, preferred_element_type=jnp.float32),
-        "ep",
-        scatter_dimension=0,
-        tiled=True,
-    )
-    dense_cols = lax.all_to_all(
-        dense_cols.astype(jnp.bfloat16), "tp", split_axis=1, concat_axis=0, tiled=True
-    ).astype(dense_cols.dtype)
-    layer_out = (
-        stream_cols.astype(jnp.float32) + expert_cols + gate_mix[:, None] * dense_cols
-    ).astype(jnp.bfloat16)
+    layer_out = layer_call(
+        heads_out,
+        residual_in,
+        norm_gain_ffn[None, :],
+        dense_mix[None, :],
+        route_ids,
+        route_weights,
+        out_weight,
+        expert_gate,
+        expert_up,
+        expert_down,
+        dense_gate,
+        dense_up,
+        dense_down,
+    )
     return (layer_out, fresh)
 
 

time: 167 us -> 56.2 us (0.34)
  blocking collectives: 82.9 us -> 0 us
  Pallas kernels: 0 us -> 39 us
  waiting for transfers between devices: 19.6 us -> 0 us
  matrix products: 24.1 us -> 8.96 us
  starting transfers between devices: 14.8 us -> 0 us
  between operations: 15 us -> 0.84 us
  other arithmetic: 6.43 us -> 3.32 us
    all_gather x3 -> x0, blocking collectives: 45.2 us -> none  [the longest x1 33.4 us: on_device(): piece = lax.all_gather(mine, 'ep', axis=0, tiled=True)]
    pallas_call x0 -> x1, Pallas kernels: none -> 39 us  [layer_call(): pl.pallas_call(functools.partial(layer_kernel, n_ep, n_tp, split), out_sh...]
    unnamed x1 -> x0, blocking collectives: 37.8 us -> none
    all_to_all x3 -> x0, starting transfers between devices: 14.7 us -> none  [the longest x1 5.98 us: on_device(): lax.all_to_all(outgoing, 'ep', split_axis=0, concat_axis=0, tiled=True)]
    dot_general x6 -> x0, matrix products: 14.4 us -> none  [the longest x1 5.08 us: on_device(): jnp.dot(dense_hidden, dense_down, preferred_element_type=jnp.float32)]
    all_to_all x3 -> x0, waiting for transfers between devices: 9.81 us -> none  [the longest x1 6.88 us: on_device(): lax.all_to_all(summed, 'ep', split_axis=0, concat_axis=0, tiled=True)]
    reduce_scatter x1 -> x0, waiting for transfers between devices: 9.79 us -> none  [on_device(): lax.psum_scatter(partial_out.astype(jnp.bfloat16), 'tp', scatter_dimensio...]
    unnamed x25 -> x23, local copies, waits for them, and re-layouts: 0.88 us -> 3.22 us
  transfers between devices with their start and end apart: 4 -> 0, of which waited for: 3 -> 0; matrix products, arithmetic and copies ran while one was open for 6% -> 0% of each run, Pallas kernels for 0% -> 0%
where the time goes in v1:
time: 56.2 us; the launch traced here: 55.8 us
  Pallas kernels  39 us (69%)
  matrix products  8.96 us (16%)
  local copies, waits for them, and re-layouts  3.7 us (7%)
  other arithmetic  3.32 us (6%)
  between operations  0.84 us (1%)
    pallas_call x1, Pallas kernels, layer_call(): pl.pallas_call(functools.partial(layer_kernel, n_ep, n_tp, split), out_sh...  39 us
    unnamed x23, local copies, waits for them, and re-layouts  3.22 us
    dot_general x1, matrix products, attend(): jnp.einsum('bgjd,bgkd->bgjk', grouped[:, :, :, 1], cache[..., QK_DIM:2 *...  2.4 us
    dot_general x1, matrix products, attend(): jnp.einsum('bgjd,bgkd->bgjk', grouped[:, :, :, 0], cache[..., :QK_DIM], p...  2.39 us
    dot_general x1, matrix products, attend(): jnp.einsum('bgjk,bgkd->bgjd', mapped, cache[..., 2 * QK_DIM:], preferred_...  2.17 us
    dot_general x1, matrix products, on_device(): jnp.dot(normed, query_weight, preferred_element_type=jnp.float32)  1.26 us

profile of v1, /device:TPU:0, one launch (start us, length us, event | category | flops | bytes accessed | tf_op | source)
XLA Modules:
  0.0 55.8 jit_solution(5248735814450329603)
XLA Ops:
  0.6 0.0 copy-start
  0.6 0.0 copy-start.8
  0.7 1.1 %fusion.14 = f32[16]{0:T(128)S(1)} fusion(bf16[16,2048]{1,0:T(8,128)(2,1)} %resid_ref.1), kind=kLoop, calls=%fused_computation.15 | loop fusion | flops 98288 | bytes 65600 | tf_op jit(solution)/shard_map/reduce_sum | solution.py:18
  1.8 0.5 copy-done
  2.3 1.3 %fusion.45 = f32[16,512]{1,0:T(8,128)S(1)} fusion(bf16[2048,512]{1,0:T(8,128)(2,1)S(1)} %copy-done, bf16[16,2048]{1,0:T(8,128)(2,1)} %resid_ref.1, f32[2048]{0:T(1024)} %param.23, f32[16]{0:T(128)S(1)} %add_rsqrt_fusion.1), kind=kOutput, calls=%fused_computation.73 | convolution fusion | flops 33685504 | bytes 2203712 | tf_op jit(solution)/shard_map/dot_general | solution.py:573
  3.5 0.1 reshape.278
  3.6 0.1 fusion.47
  3.8 0.0 copy-done.8
  3.8 0.1 multiply_cosine_fusion
  4.0 0.1 fusion.33
  4.1 0.0 copy-start.1
  4.1 0.0 copy-start.2
  4.1 0.0 copy-start.4
  4.1 2.4 %fusion.10 = f32[16,4,512]{2,1,0:T(4,128)S(1)} fusion(bf16[16,4,64]{2,1,0:T(4,128)(2,1)S(1)} %get-tuple-element.8, bf16[16,1,512,256]{3,2,1,0:T(8,128)(2,1)} %param.22), kind=kOutput, calls=%fused_computation.9 | convolution fusion | flops 4227072 | bytes 2236416 | tf_op jit(solution)/shard_map/bgjd,bgkd->bgjk/dot_general | solution.py:60
  6.5 0.0 copy-start.7
  6.5 0.0 copy-start.3
  6.5 0.1 iota_compare_fusion
  6.6 2.4 %select_reduce_fusion.1 = (f32[16,4]{1,0:T(8,128)S(1)}, f32[16,4]{1,0:T(8,128)S(1)}, f32[16,4,512]{2,1,0:T(4,128)S(1)}) fusion(pred[16,512]{1,0:T(8,128)(4,1)S(1)} %iota_compare_fusion, f32[16,4,512]{2,1,0:T(4,128)S(1)} %fusion.10, bf16[16,4,64]{2,1,0:T(4,128)(2,1)S(1)} %get-tuple-element.9, bf16[16,1,512,256]{3,2,1,0:T(8,128)(2,1)} %param.22), kind=kOutput, calls=%fused_computation.21 | convolution fusion | flops 4358016 | bytes 2376192 | tf_op jit(solution)/shard_map/bgjd,bgkd->bgjk/dot_general | solution.py:51
  9.0 0.0 copy-done.1
  9.0 0.0 copy-done.2
  9.0 0.0 copy-done.4
  9.0 0.2 fusion.43
  9.2 0.1 reshape.281
  9.3 0.1 subtract_convert_fusion.1
  9.4 0.1 pad_maximum_fusion.1
  9.5 0.1 convert_element_type.61
  9.6 0.1 slice_bitcast_fusion.4
  9.7 0.1 fusion.34
  9.8 0.1 fusion.36
  10.0 0.3 fusion.18
  10.3 0.0 copy-done.7
  10.3 0.0 copy-done.3
  10.3 0.2 fusion.48
  10.6 0.0 copy-start.9
  10.6 0.0 copy-start.5
  10.6 0.0 copy-start.6
  10.6 2.2 %multiply_reduce_fusion = (f32[16,4]{1,0:T(8,128)S(1)}, f32[16,4,128]{2,1,0:T(4,128)S(1)}) fusion(f32[16,128]{1,0:T(8,128)S(1)} %get-tuple-element.22, f32[16,4]{1,0:T(8,128)S(1)} %get-tuple-element.14, bf16[16,1,512,256]{3,2,0,1:T(8,128)(2,1)} %bitcast.59, f32[16,4,512]{2,1,0:T(4,128)S(1)} %get-tuple-element.21, f32[16,4,512]{2,1,0:T(4,128)S(1)} %fusion.10, ...), kind=kOutput, calls=%fused_computation.38 | convolution fusion | flops 8781760 | bytes 2410000 | tf_op jit(solution)/shard_map/bgjk,bgkd->bgjd/dot_general | solution.py:95
  12.8 0.1 broadcast_multiply_fusion
  12.9 0.0 copy-done.9
  12.9 0.6 %fusion.28.heads_ref = bf16[16,512]{1,0:T(8,128)(2,1)} fusion(f32[2,8,4,128]{3,2,1,0:T(4,128)S(1)} %bitcast.60, f32[512]{0:T(512)S(1)} %broadcast_bitcast_fusion), kind=kLoop, calls=%fused_computation.35 | loop fusion | flops 16384 | bytes 51200 | tf_op jit(solution)/shard_map/convert_element_type | solution.py:589
  13.5 0.0 copy-done.5
  13.5 0.7 %copy.27.ids_ref = s32[16,2]{1,0:T(8,128)} copy(s32[16,2]{0,1:T(2,128)S(1)} %copy-done.5) | data formatting | bytes 256 | tf_op args[11]
  14.2 0.0 copy-done.6
  14.2 0.7 %copy.28.rw_ref = f32[16,2]{1,0:T(8,128)} copy(f32[16,2]{0,1:T(2,128)S(1)} %copy-done.6) | data formatting | bytes 256 | tf_op args[12]
  14.9 39.0 %shard_map.203 = bf16[16,512]{1,0:T(8,128)(2,1)} custom-call(bf16[16,512]{1,0:T(8,128)(2,1)} %fusion.28.heads_ref, bf16[16,2048]{1,0:T(8,128)(2,1)} %resid_ref.1, f32[1,2048]{1,0:T(1,128)} %bitcast.66, f32[1,2048]{1,0:T(1,128)} %bitcast.67, s32[16,2]{1,0:T(8,128)} %copy.27.ids_ref, f32[16,2]{1,0:T(8,128)} %copy.28.rw_ref, bf16[2048,512]{1,0:T(8,128)(2,1)} %ow_hbm.1, ...), custom_call_target="tpu_custom_call" | custom-call | tf_op jit(solution)/shard_map/pallas_call | solution.py:501
  53.9 0.6 %pad_maximum_fusion.2 = bf16[16,1,256]{2,0,1:T(8,128)(2,1)} fusion(bf16[16,1,128]{2,0,1:T(8,128)(2,1)S(1)} %bitcast.65, bf16[16,1,128]{2,0,1:T(8,128)(2,1)S(1)} %convert_element_type.61), kind=kLoop, calls=%fused_computation.52 | loop fusion | flops 16384 | bytes 16384 | tf_op jit(solution)/shard_map/concatenate | solution.py:586
  54.5 1.3 %copy.56 = bf16[16,512]{1,0:T(8,128)(2,1)} copy(bf16[16,512]{1,0:T(8,128)(2,1)} %shard_map.203) | data formatting | bytes 32768
  (8 shorter events, 0.1 us)
Async XLA Ops:
  0.6 1.6 %copy-start = (bf16[2048,512]{1,0:T(8,128)(2,1)S(1)}, bf16[2048,512]{1,0:T(8,128)(2,1)}, u32[]{:S(2)}) copy-start(bf16[2048,512]{1,0:T(8,128)(2,1)} %param.24) | copy-start | bytes 6291460
  0.6 3.1 %copy-start.8 = (s32[16]{0:T(128)S(1)}, s32[16]{0:T(128)}, u32[]{:S(2)}) copy-start(s32[16]{0:T(128)} %param.21) | copy-start | bytes 196
  4.1 4.9 %copy-start.1 = (bf16[16,2048]{1,0:T(8,128)(2,1)S(1)}, bf16[16,2048]{1,0:T(8,128)(2,1)}, u32[]{:S(2)}) copy-start(bf16[16,2048]{1,0:T(8,128)(2,1)} %resid_ref.1) | copy-start | bytes 196612
  4.1 4.9 %copy-start.2 = (bf16[2048,128]{1,0:T(8,128)(2,1)S(1)}, bf16[2048,128]{1,0:T(8,128)(2,1)}, u32[]{:S(2)}) copy-start(bf16[2048,128]{1,0:T(8,128)(2,1)} %param.25) | copy-start | bytes 1572868
  4.1 4.9 %copy-start.4 = (f32[2048]{0:T(1024)S(1)}, f32[2048]{0:T(1024)}, u32[]{:S(2)}) copy-start(f32[2048]{0:T(1024)} %param.23) | copy-start | bytes 24580
  6.5 3.8 %copy-start.7 = (f32[4]{0:T(128)S(1)}, f32[4]{0:T(128)}, u32[]{:S(2)}) copy-start(f32[4]{0:T(128)} %param.27) | copy-start | bytes 52
  6.5 3.8 %copy-start.3 = (bf16[2048,128]{1,0:T(8,128)(2,1)S(1)}, bf16[2048,128]{1,0:T(8,128)(2,1)}, u32[]{:S(2)}) copy-start(bf16[2048,128]{1,0:T(8,128)(2,1)} %param.26) | copy-start | bytes 1572868
  10.6 2.3 %copy-start.9 = (f32[128]{0:T(128)S(1)}, f32[128]{0:T(128)}, u32[]{:S(2)}) copy-start(f32[128]{0:T(128)} %param.28) | copy-start | bytes 1540
  10.6 2.9 %copy-start.5 = (s32[16,2]{0,1:T(2,128)S(1)}, s32[16,2]{0,1:T(2,128)}, u32[]{:S(2)}) copy-start(s32[16,2]{0,1:T(2,128)} %param.31) | copy-start | bytes 388
  10.6 3.6 %copy-start.6 = (f32[16,2]{0,1:T(2,128)S(1)}, f32[16,2]{0,1:T(2,128)}, u32[]{:S(2)}) copy-start(f32[16,2]{0,1:T(2,128)} %param.32) | copy-start | bytes 388

commit v2 on v1

--- a/solution.py
+++ b/solution.py
@@ -1,4 +1,5 @@
 import functools
+import math
 
 import jax
 import jax.numpy as jnp
@@ -8,103 +9,12 @@
 from jax.sharding import PartitionSpec as P
 
 QK_DIM = 64
-HEAD_DIM = 128
-
-
 EPS = 1e-06
-
-
-def rms_rows(values, gain):
-    mean_sq = jnp.mean(values * values, axis=-1, keepdims=True)
-    return values * lax.rsqrt(mean_sq + EPS) * gain
-
-
-def rotate(vectors, positions):
-    half = vectors.shape[-1] // 2
-    inverse = 10000.0 ** (-jnp.arange(half, dtype=jnp.float32) / half)
-    angle = positions[:, None, None, None] * inverse
-    cosine = jnp.cos(angle)
-    sine = jnp.sin(angle)
-    first = vectors[..., :half]
-    second = vectors[..., half:]
-    return jnp.concatenate(
-        [first * cosine - second * sine, first * sine + second * cosine], axis=-1
-    )
-
-
-def normalize(scores, latest, valid):
-    masked = jnp.where(valid, scores, -jnp.inf)
-    top = jnp.maximum(jnp.max(masked, axis=-1), latest)
-    raised = jnp.where(valid, jnp.exp(jnp.where(valid, scores, 0.0) - top[..., None]), 0.0)
-    raised_new = jnp.exp(latest - top)
-    total = jnp.sum(raised, axis=-1) + raised_new
-    return (raised / total[..., None], raised_new / total)
-
-
-def attend(query, fresh, cache, lengths, lam):
-    count = fresh.shape[0]
-    groups = fresh.shape[1]
-    share = query.shape[1] // groups
-    scale = QK_DIM ** (-0.5)
-    grouped = query.reshape(count, groups, share, 2, QK_DIM)
-    first = (
-        jnp.einsum(
-            "bgjd,bgkd->bgjk",
-            grouped[:, :, :, 0],
-            cache[..., :QK_DIM],
-            preferred_element_type=jnp.float32,
-        )
-        * scale
-    )
-    second = (
-        jnp.einsum(
-            "bgjd,bgkd->bgjk",
-            grouped[:, :, :, 1],
-            cache[..., QK_DIM : 2 * QK_DIM],
-            preferred_element_type=jnp.float32,
-        )
-        * scale
-    )
-    first_new = (
-        jnp.einsum(
-            "bgjd,bgd->bgj",
-            grouped[:, :, :, 0],
-            fresh[..., :QK_DIM],
-            preferred_element_type=jnp.float32,
-        )
-        * scale
-    )
-    second_new = (
-        jnp.einsum(
-            "bgjd,bgd->bgj",
-            grouped[:, :, :, 1],
-            fresh[..., QK_DIM : 2 * QK_DIM],
-            preferred_element_type=jnp.float32,
-        )
-        * scale
-    )
-    valid = (
-        jnp.arange(cache.shape[2], dtype=jnp.int32)[None, None, None, :]
-        < lengths[:, None, None, None]
-    )
-    prob_one, prob_one_new = normalize(first, first_new, valid)
-    prob_two, prob_two_new = normalize(second, second_new, valid)
-    weight = lam.reshape(groups, share)[None, :, :, None]
-    mapped = (prob_one - weight * prob_two).astype(jnp.bfloat16)
-    mapped_new = (prob_one_new - weight[..., 0] * prob_two_new).astype(jnp.bfloat16)
-    output = jnp.einsum(
-        "bgjk,bgkd->bgjd", mapped, cache[..., 2 * QK_DIM :], preferred_element_type=jnp.float32
-    )
-    output = output + mapped_new.astype(jnp.float32)[..., None] * fresh[
-        :, :, None, 2 * QK_DIM :
-    ].astype(jnp.float32)
-    return output.reshape(count, groups * share, HEAD_DIM)
-
-
 MESH = pl.DeviceIdType.MESH
 F32 = jnp.float32
 BF16 = jnp.bfloat16
 LANES = 128
+Q_CHUNKS = 4
 
 
 def flip(value, mask):
@@ -148,16 +58,30 @@
     return jnp.dot(left, right, preferred_element_type=F32)
 
 
+def column(row):
+    count = row.shape[1]
+    square = (count, count)
+    same = lax.broadcasted_iota(jnp.int32, square, 0) == lax.broadcasted_iota(jnp.int32, square, 1)
+    return jnp.sum(jnp.where(same, row, jnp.zeros_like(row)), axis=1, keepdims=True)
+
+
 def layer_kernel(
     n_ep,
     n_tp,
     split,
-    heads_ref,
+    lengths_ref,
+    lam_ref,
     resid_ref,
+    first_gain_ref,
+    head_gain_ref,
     gain_ref,
     mixw_ref,
     ids_ref,
     rw_ref,
+    qw_hbm,
+    kw_hbm,
+    vw_hbm,
+    cache_hbm,
     ow_hbm,
     eg_hbm,
     eu_hbm,
@@ -166,6 +90,15 @@
     du_hbm,
     dd_hbm,
     out_ref,
+    new_ref,
+    qw,
+    kw,
+    vw,
+    cache,
+    pairs,
+    scores,
+    mixed,
+    heads_ref,
     ow,
     eg,
     eu,
@@ -185,6 +118,8 @@
     summed,
     landed,
     w_sem,
+    q_sem,
+    cache_sem,
     route_send,
     route_recv,
     heads_send,
@@ -210,6 +145,24 @@
     rows_all = n_ep * seqs
     evens = [2 * i for i in range(1, half)]
 
+    depth = qw.shape[0] // Q_CHUNKS
+    q_loads = [
+        pltpu.make_async_copy(
+            qw_hbm.at[pl.ds(i * depth, depth), :], qw.at[pl.ds(i * depth, depth), :], q_sem.at[i]
+        )
+        for i in range(Q_CHUNKS)
+    ] + [
+        pltpu.make_async_copy(kw_hbm, kw, q_sem.at[Q_CHUNKS]),
+        pltpu.make_async_copy(vw_hbm, vw, q_sem.at[Q_CHUNKS + 1]),
+    ]
+    for load in q_loads:
+        load.start()
+    cache_loads = [
+        pltpu.make_async_copy(cache_hbm.at[s], cache.at[s], cache_sem.at[s]) for s in range(seqs)
+    ]
+    for load in cache_loads:
+        load.start()
+
     barrier = pltpu.get_barrier_semaphore()
 
     def greet(index):
@@ -236,29 +189,65 @@
             zip((ow_hbm, eg_hbm, eu_hbm) + dense_parts[:2] + (ed_hbm, dense_parts[2]), (ow, eg, eu, dg, du, ed, dd))
         )
     ]
+
+    lane = lax.broadcasted_iota(jnp.int32, (seqs, route.shape[1]), 1)
+    table = jnp.zeros((seqs, route.shape[1]), F32)
+    for k in range(ids_ref.shape[0]):
+        wanted = column(ids_ref[k : k + 1, :])
+        table = table + jnp.where(lane == wanted, column(rw_ref[k : k + 1, :]), 0.0)
+    own_rows = block(e, seqs)
+    route[own_rows, :] = table
+
+    resid = resid_ref[...].astype(F32)
+    mean_sq = jnp.mean(resid * resid, axis=-1, keepdims=True)
+    normed = (resid * lax.rsqrt(mean_sq + EPS) * first_gain_ref[...]).astype(BF16)
+    row = lax.broadcasted_iota(jnp.int32, (seqs, LANES), 0)
+    entry = lax.broadcasted_iota(jnp.int32, (seqs, LANES), 1) % QK_DIM
+    position = jnp.zeros((seqs, LANES), F32)
+    for s in range(seqs):
+        position = jnp.where(row == s, lengths_ref[s].astype(F32), position)
+    turn = QK_DIM // 2
+    power = (entry % turn).astype(F32) * (-1.0 / turn)
+    angle = position * jnp.exp(power * math.log(10000.0))
+    cosine = jnp.cos(angle)
+    sine = jnp.where(entry < turn, -jnp.sin(angle), jnp.sin(angle))
+
+    def rotate(values):
+        other = jnp.where(
+            entry < turn, pltpu.roll(values, LANES - turn, 1), pltpu.roll(values, turn, 1)
+        )
+        return (values * cosine + other * sine).astype(BF16).astype(F32)
+
+    query = jnp.zeros((seqs, qw.shape[1]), F32)
+    for i in range(Q_CHUNKS):
+        q_loads[i].wait()
+        query = query + dot(
+            normed[:, i * depth : (i + 1) * depth], qw[i * depth : (i + 1) * depth, :]
+        )
+    for load in q_loads[Q_CHUNKS:]:
+        load.wait()
+    keys_raw = dot(normed, kw[...])
+    values_raw = dot(normed, vw[...])
     for load in loads:
         load.start()
 
-    lane = lax.broadcasted_iota(jnp.int32, (seqs, route.shape[1]), 1)
-    table = jnp.zeros((seqs, route.shape[1]), F32)
-    for k in range(ids_ref.shape[1]):
-        table = table + jnp.where(lane == ids_ref[:, k : k + 1], rw_ref[:, k : k + 1], 0.0)
-    own_rows = block(e, seqs)
-    route[own_rows, :] = table
+    groups, spots = cache.shape[1], cache.shape[2]
+    share = query.shape[1] // LANES // groups
+    lower = lax.broadcasted_iota(jnp.int32, (seqs, LANES), 1) < QK_DIM
+    fresh = []
+    for g in range(groups):
+        key = rotate(keys_raw[:, g * LANES : (g + 1) * LANES])
+        value = values_raw[:, g * LANES : (g + 1) * LANES].astype(BF16).astype(F32)
+        new_ref[:, 2 * g * LANES : (2 * g + 1) * LANES] = key
+        new_ref[:, (2 * g + 1) * LANES : (2 * g + 2) * LANES] = value
+        fresh.append((key, value))
+        for j in range(share):
+            at = (g * share + j) * LANES
+            head = rotate(query[:, at : at + LANES])
+            pairs[g, :, j, :] = jnp.where(lower, head, 0.0)
+            pairs[g, :, share + j, :] = jnp.where(lower, 0.0, head)
 
     pl.semaphore_wait(barrier, n_ep * half - 1 + half)
-
-    def heads_copy(mask):
-        return remote(
-            heads_ref,
-            heads_all.at[mask - 1],
-            heads_send.at[mask - 1],
-            heads_recv.at[mask - 1],
-            (e, flip(t, mask)),
-        )
-
-    for mask in range(n_tp - 1, 0, -1):
-        heads_copy(mask).start()
 
     def route_copy(d):
         there = (e + d) % n_ep
@@ -276,6 +265,65 @@
         remote(spot, spot, route_send.at[d - 1], route_recv.at[d - 1], (e, t)).wait_recv()
 
     each(n_ep - 1, lambda i: route_copy(i + 1).start())
+
+    scale = QK_DIM**-0.5
+    lines = 2 * share
+    for s in range(seqs):
+        cache_loads[s].wait()
+        for g in range(groups):
+            both = pairs[g, s].astype(BF16)
+            scores[g, s] = (
+                lax.dot_general(
+                    both,
+                    cache[s, g, :, :LANES],
+                    (((1,), (1,)), ((), ())),
+                    preferred_element_type=F32,
+                )
+                * scale
+            )
+    length = jnp.zeros((seqs, lines, 1), jnp.int32)
+    which = lax.broadcasted_iota(jnp.int32, (seqs, lines, 1), 0)
+    for s in range(seqs):
+        length = jnp.where(which == s, lengths_ref[s], length)
+    place = lax.broadcasted_iota(jnp.int32, (seqs, lines, spots), 2)
+    valid = place < length
+    line = lax.broadcasted_iota(jnp.int32, (lines, 1), 0)
+    for g in range(groups):
+        key, value = fresh[g]
+        latest = jnp.sum(pairs[g] * key[:, None, :], axis=-1, keepdims=True) * scale
+        masked = jnp.where(valid, scores[g], -jnp.inf)
+        top = jnp.maximum(jnp.max(masked, axis=-1, keepdims=True), latest)
+        raised = jnp.exp(masked - top)
+        raised_new = jnp.exp(latest - top)
+        total = jnp.sum(raised, axis=-1, keepdims=True) + raised_new
+        prob = raised / total
+        prob_new = jnp.broadcast_to(raised_new / total, (seqs, lines, LANES))
+        lam = jnp.zeros((lines, 1), F32)
+        for j in range(share):
+            lam = jnp.where(line == j, lam_ref[g * share + j], lam)
+        scores[g] = prob - lam[None] * pltpu.roll(prob, share, 1)
+        new_weight = (prob_new - lam[None] * pltpu.roll(prob_new, share, 1)).astype(BF16).astype(F32)
+        fresh_part = new_weight * value[:, None, :]
+        for s in range(seqs):
+            mixed[g, s] = dot(scores[g, s].astype(BF16), cache[s, g, :, LANES:])
+        whole = mixed[g] + fresh_part
+        mean_sq = jnp.mean(whole * whole, axis=-1, keepdims=True)
+        mixed[g] = whole * lax.rsqrt(mean_sq + EPS) * head_gain_ref[...][None]
+        for j in range(share):
+            at = (g * share + j) * LANES
+            heads_ref[:, at : at + LANES] = mixed[g, :, j, :].astype(BF16)
+
+    def heads_copy(mask):
+        return remote(
+            heads_ref,
+            heads_all.at[mask - 1],
+            heads_send.at[mask - 1],
+            heads_recv.at[mask - 1],
+            (e, flip(t, mask)),
+        )
+
+    for mask in range(n_tp - 1, 0, -1):
+        heads_copy(mask).start()
 
     loads[0].wait()
     span = heads_ref.shape[1]
@@ -456,9 +504,7 @@
             remote(where, where, back_send.at[0, 0], back_recv.at[index], (e, t)).wait_recv()
 
     each(n_ep * half, take)
-    out_ref[...] = (
-        own_stream.astype(F32) + jnp.sum(landed[...].astype(F32), axis=0)
-    ).astype(BF16)
+    out_ref[...] = own_stream.astype(F32) + jnp.sum(landed[...].astype(F32), axis=0)
 
     for mask in range(1, n_tp):
         heads_copy(mask).wait_send()
@@ -481,65 +527,6 @@
                 back(j, d).wait_send()
 
         each(n_ep, gone)
-
-
-def layer_call(heads, resid, gain, mixw, ids, rw, ow, eg, eu, ed, dg, du, dd):
-    n_ep = lax.axis_size("ep")
-    n_tp = lax.axis_size("tp")
-    half = n_tp // 2
-    seqs, width = resid.shape
-    quarter = ow.shape[1]
-    held, _, part = eg.shape
-    rows = n_ep * seqs
-    own = dg.shape[1] // n_tp
-    split = own % LANES == 0
-    hid = own if split else dg.shape[1]
-    lanes = -(-n_ep * held // LANES) * LANES
-    vmem = pl.BlockSpec(memory_space=pltpu.VMEM)
-    hbm = pl.BlockSpec(memory_space=pl.ANY)
-    dma = pltpu.SemaphoreType.DMA
-    return pl.pallas_call(
-        functools.partial(layer_kernel, n_ep, n_tp, split),
-        out_shape=jax.ShapeDtypeStruct((seqs, quarter), BF16),
-        in_specs=[vmem] * 6 + [hbm] * 7,
-        out_specs=vmem,
-        scratch_shapes=[
-            pltpu.VMEM(ow.shape, BF16),
-            pltpu.VMEM(eg.shape, BF16),
-            pltpu.VMEM(eu.shape, BF16),
-            pltpu.VMEM(ed.shape, BF16),
-            pltpu.VMEM((width, hid), BF16),
-            pltpu.VMEM((width, hid), BF16),
-            pltpu.VMEM((hid, width), BF16),
-            pltpu.VMEM((n_tp - 1,) + heads.shape, BF16),
-            pltpu.VMEM((rows, width), BF16),
-            pltpu.VMEM((rows, width), BF16),
-            pltpu.VMEM((rows, LANES), F32),
-            pltpu.VMEM((rows, lanes), F32),
-            pltpu.VMEM((held, rows, part), BF16),
-            pltpu.VMEM((rows, hid), BF16),
-            pltpu.VMEM((half, rows, quarter), BF16),
-            pltpu.VMEM((half, rows, quarter), BF16),
-            pltpu.VMEM((half, rows, quarter), BF16),
-            pltpu.VMEM((n_ep * half, seqs, quarter), BF16),
-            dma((7,)),
-            dma((n_ep - 1,)),
-            dma((n_ep - 1,)),
-            dma((n_tp - 1,)),
-            dma((n_tp - 1,)),
-            dma((n_ep,)),
-            dma((half, n_ep)),
-            dma((max(half - 1, 1), n_ep)),
-            dma((n_tp, n_ep)),
-            dma((half,)),
-            dma((half,)),
-            dma((half, n_ep)),
-            dma((n_ep * half,)),
-        ],
-        compiler_params=pltpu.CompilerParams(
-            collective_id=0, has_side_effects=True, vmem_limit_bytes=56 * 1024 * 1024
-        ),
-    )(heads, resid, gain, mixw, ids, rw, ow, eg, eu, ed, dg, du, dd)
 
 
 def on_device(
@@ -564,37 +551,92 @@
     dense_down,
     dense_mix,
 ):
-    seq_count, width = residual_in.shape
-    groups = kv_cache.shape[1]
-    local_heads = diff_lambda.shape[0]
-    resid = residual_in.astype(jnp.float32)
-    normed = rms_rows(resid, norm_gain_attn).astype(jnp.bfloat16)
-    positions = lengths.astype(jnp.float32)
-    query = jnp.dot(normed, query_weight, preferred_element_type=jnp.float32).reshape(
-        seq_count, local_heads, 2, QK_DIM
-    )
-    query = rotate(query, positions).astype(jnp.bfloat16)
-    keys = jnp.dot(normed, key_weight, preferred_element_type=jnp.float32).reshape(
-        seq_count, groups, 2, QK_DIM
-    )
-    keys = rotate(keys, positions).astype(jnp.bfloat16).reshape(seq_count, groups, 2 * QK_DIM)
-    values = (
-        jnp.dot(normed, value_weight, preferred_element_type=jnp.float32)
-        .reshape(seq_count, groups, HEAD_DIM)
-        .astype(jnp.bfloat16)
-    )
-    fresh = jnp.concatenate([keys, values], axis=-1)
-    mixed = attend(query, fresh, kv_cache, lengths, diff_lambda)
-    heads_out = (
-        rms_rows(mixed, head_gain).astype(jnp.bfloat16).reshape(seq_count, local_heads * HEAD_DIM)
-    )
-    layer_out = layer_call(
-        heads_out,
+    n_ep = lax.axis_size("ep")
+    n_tp = lax.axis_size("tp")
+    half = n_tp // 2
+    seqs, width = residual_in.shape
+    groups, spots = kv_cache.shape[1:3]
+    share = diff_lambda.shape[0] // groups
+    inner = query_weight.shape[1]
+    quarter = out_weight.shape[1]
+    held, _, part = expert_gate.shape
+    rows = n_ep * seqs
+    own = dense_gate.shape[1] // n_tp
+    split = own % LANES == 0
+    hid = own if split else dense_gate.shape[1]
+    lanes = -(-n_ep * held // LANES) * LANES
+    vmem = pl.BlockSpec(memory_space=pltpu.VMEM)
+    smem = pl.BlockSpec(memory_space=pltpu.SMEM)
+    hbm = pl.BlockSpec(memory_space=pl.ANY)
+    dma = pltpu.SemaphoreType.DMA
+    layer_out, fresh = pl.pallas_call(
+        functools.partial(layer_kernel, n_ep, n_tp, split),
+        out_shape=(
+            jax.ShapeDtypeStruct((seqs, quarter), F32),
+            jax.ShapeDtypeStruct((seqs, groups * kv_cache.shape[3]), F32),
+        ),
+        in_specs=[smem] * 2 + [vmem] * 7 + [hbm] * 11,
+        out_specs=(vmem, vmem),
+        scratch_shapes=[
+            pltpu.VMEM(query_weight.shape, BF16),
+            pltpu.VMEM(key_weight.shape, BF16),
+            pltpu.VMEM(value_weight.shape, BF16),
+            pltpu.VMEM(kv_cache.shape, BF16),
+            pltpu.VMEM((groups, seqs, 2 * share, LANES), F32),
+            pltpu.VMEM((groups, seqs, 2 * share, spots), F32),
+            pltpu.VMEM((groups, seqs, 2 * share, LANES), F32),
+            pltpu.VMEM((seqs, inner), BF16),
+            pltpu.VMEM(out_weight.shape, BF16),
+            pltpu.VMEM(expert_gate.shape, BF16),
+            pltpu.VMEM(expert_up.shape, BF16),
+            pltpu.VMEM(expert_down.shape, BF16),
+            pltpu.VMEM((width, hid), BF16),
+            pltpu.VMEM((width, hid), BF16),
+            pltpu.VMEM((hid, width), BF16),
+            pltpu.VMEM((n_tp - 1, seqs, inner), BF16),
+            pltpu.VMEM((rows, width), BF16),
+            pltpu.VMEM((rows, width), BF16),
+            pltpu.VMEM((rows, LANES), F32),
+            pltpu.VMEM((rows, lanes), F32),
+            pltpu.VMEM((held, rows, part), BF16),
+            pltpu.VMEM((rows, hid), BF16),
+            pltpu.VMEM((half, rows, quarter), BF16),
+            pltpu.VMEM((half, rows, quarter), BF16),
+            pltpu.VMEM((half, rows, quarter), BF16),
+            pltpu.VMEM((n_ep * half, seqs, quarter), BF16),
+            dma((7,)),
+            dma((Q_CHUNKS + 2,)),
+            dma((seqs,)),
+            dma((n_ep - 1,)),
+            dma((n_ep - 1,)),
+            dma((n_tp - 1,)),
+            dma((n_tp - 1,)),
+            dma((n_ep,)),
+            dma((half, n_ep)),
+            dma((max(half - 1, 1), n_ep)),
+            dma((n_tp, n_ep)),
+            dma((half,)),
+            dma((half,)),
+            dma((half, n_ep)),
+            dma((n_ep * half,)),
+        ],
+        compiler_params=pltpu.CompilerParams(
+            collective_id=0, has_side_effects=True, vmem_limit_bytes=60 * 1024 * 1024
+        ),
+    )(
+        lengths,
+        diff_lambda,
         residual_in,
+        norm_gain_attn[None, :],
+        head_gain[None, :],
         norm_gain_ffn[None, :],
         dense_mix[None, :],
-        route_ids,
-        route_weights,
+        route_ids.T,
+        route_weights.T,
+        query_weight,
+        key_weight,
+        value_weight,
+        kv_cache,
         out_weight,
         expert_gate,
         expert_up,
@@ -603,7 +645,8 @@
         dense_up,
         dense_down,
     )
-    return (layer_out, fresh)
+    new_rows = fresh.astype(BF16).reshape(seqs, groups, kv_cache.shape[3])
+    return (layer_out.astype(BF16), new_rows)
 
 
 def solution(mesh):

time: 56.2 us -> 46 us (0.82)
  matrix products: 8.96 us -> 0 us
  local copies, waits for them, and re-layouts: 3.7 us -> 0 us
  Pallas kernels: 39 us -> 42.4 us
  other arithmetic: 3.32 us -> 2.68 us
    dot_general x8 -> x0, matrix products: 8.96 us -> none  [the longest x1 2.4 us: attend(): jnp.einsum('bgjd,bgkd->bgjk', grouped[:, :, :, 1], cache[..., QK_DIM:2 *...]
    pallas_call x1, Pallas kernels: 39 us -> 42.4 us  [on_device(): pl.pallas_call(functools.partial(layer_kernel, n_ep, n_tp, split), out_sh...]
    unnamed x23 -> x0, local copies, waits for them, and re-layouts: 3.22 us -> none
    reduce_sum x2 -> x0, other arithmetic: 1.43 us -> none  [the longest x1 1.11 us: rms_rows(): mean_sq = jnp.mean(values * values, axis=-1, keepdims=True)]
    reshape x0 -> x1, other arithmetic: none -> 1.32 us  [on_device(): new_rows = fresh.astype(BF16).reshape(seqs, groups, kv_cache.shape[3])]
    concatenate x3 -> x0, other arithmetic: 0.73 us -> none  [the longest x1 0.6 us: on_device(): fresh = jnp.concatenate([keys, values], axis=-1)]
    convert_element_type x3 -> x1, other arithmetic: 0.64 us -> 1.37 us  [on_device(): return (layer_out.astype(BF16), new_rows)]
where the time goes in v2:
time: 46 us; the launch traced here: 45.7 us
  Pallas kernels  42.4 us (92%)
  other arithmetic  2.68 us (6%)
  between operations  0.65 us (1%)
    pallas_call x1, Pallas kernels, on_device(): pl.pallas_call(functools.partial(layer_kernel, n_ep, n_tp, split), out_sh...  42.4 us
    convert_element_type x1, other arithmetic, on_device(): return (layer_out.astype(BF16), new_rows)  1.37 us
    reshape x1, other arithmetic, on_device(): new_rows = fresh.astype(BF16).reshape(seqs, groups, kv_cache.shape[3])  1.32 us

profile of v2, /device:TPU:0, one launch (start us, length us, event | category | flops | bytes accessed | tf_op | source)
XLA Modules:
  0.0 45.7 jit_solution(15091195352521071757)
XLA Ops:
  0.6 42.4 %shard_map.203 = (f32[16,512]{1,0:T(8,128)}, f32[16,256]{1,0:T(8,128)}) custom-call(s32[16]{0:T(128)} %lengths_ref.1, f32[4]{0:T(128)} %lam_ref.1, bf16[16,2048]{1,0:T(8,128)(2,1)} %resid_ref.1, f32[1,2048]{1,0:T(1,128)} %bitcast.8, f32[1,128]{1,0:T(1,128)} %bitcast.13, f32[1,2048]{1,0:T(1,128)} %bitcast.9, f32[1,2048]{1,0:T(1,128)} %bitcast.10, ...), custom_call_target="tpu_custom_call" | custom-call | tf_op jit(solution)/shard_map/pallas_call | solution.py:572
  43.0 1.4 %convert_element_type.6 = bf16[16,512]{1,0:T(8,128)(2,1)} convert(f32[16,512]{1,0:T(8,128)} %get-tuple-element.4) | non-fusion elementwise | flops 8192 | bytes 49152 | tf_op jit(solution)/shard_map/convert_element_type | solution.py:649
  44.4 1.3 %convert_bitcast_fusion = bf16[16,1,256]{2,0,1:T(8,128)(2,1)} fusion(f32[16,256]{1,0:T(8,128)} %get-tuple-element.5), kind=kLoop, calls=%fused_computation | loop fusion | flops 4096 | bytes 24576 | tf_op jit(solution)/shard_map/reshape | solution.py:648

commit v3 on v2

--- a/solution.py
+++ b/solution.py
@@ -116,6 +116,7 @@
     away,
     came,
     summed,
+    crossed,
     landed,
     w_sem,
     q_sem,
@@ -130,6 +131,8 @@
     stream_recv,
     pair_send,
     pair_recv,
+    cross_send,
+    cross_recv,
     back_send,
     back_recv,
 ):
@@ -137,7 +140,6 @@
     t = lax.axis_index("tp")
     half = n_tp // 2
     mate = flip(t, 1)
-    core = t % 2
     seqs, width = resid_ref.shape
     quarter = out_ref.shape[1]
     held, _, part = eg.shape
@@ -166,17 +168,13 @@
     barrier = pltpu.get_barrier_semaphore()
 
     def greet(index):
-        where = (index // half, 2 * (index % half) + core)
-
-        @pl.when(jnp.logical_or(where[0] != e, where[1] != t))
-        def _():
-            pl.semaphore_signal(barrier, inc=1, device_id=where, device_id_type=MESH)
-
-    each(n_ep * half, greet)
-    for i in range(half):
         pl.semaphore_signal(
-            barrier, inc=1, device_id=(e, 2 * i + 1 - core), device_id_type=MESH
-        )
+            barrier, inc=1, device_id=((e + index + 1) % n_ep, t), device_id_type=MESH
+        )
+
+    each(n_ep - 1, greet)
+    for mask in range(1, n_tp):
+        pl.semaphore_signal(barrier, inc=1, device_id=(e, flip(t, mask)), device_id_type=MESH)
 
     if split:
         cols = block(t, hid)
@@ -247,7 +245,7 @@
             pairs[g, :, j, :] = jnp.where(lower, head, 0.0)
             pairs[g, :, share + j, :] = jnp.where(lower, 0.0, head)
 
-    pl.semaphore_wait(barrier, n_ep * half - 1 + half)
+    pl.semaphore_wait(barrier, n_ep + n_tp - 2)
 
     def route_copy(d):
         there = (e + d) % n_ep
@@ -450,61 +448,76 @@
     def pair(j):
         return remote(away.at[j], came.at[j], pair_send.at[j], pair_recv.at[j], (e, mate))
 
-    for j in range(half):
-
-        def leave(b, j=j):
-            away[j, block(b, many), :] = result(b, 2 * j + 1 - core).astype(BF16)
+    masks = evens + [0]
+    for j, mask in enumerate(masks):
+
+        def leave(b, j=j, mask=mask):
+            away[j, block(b, many), :] = result(b, flip(mate, mask)).astype(BF16)
 
         each(batches, leave)
         pair(j).start()
 
-    me = e * half + t // 2
-
-    def back(j, d):
+    def cross(j, d):
+        rows = block((e + d) % n_ep, seqs)
+        return remote(
+            summed.at[j, rows, :],
+            crossed.at[j, rows, :],
+            cross_send.at[j, d],
+            cross_recv.at[j, d],
+            (e, flip(t, masks[j])),
+        )
+
+    final = half - 1
+
+    def back(d):
         there = (e + d) % n_ep
         return remote(
-            summed.at[j, block(there, seqs), :],
-            landed.at[me],
-            back_send.at[j, d],
-            back_recv.at[me],
-            (there, 2 * j + core),
-        )
-
-    def same(j, d):
-        return jnp.logical_and(jnp.asarray(d == 0), 2 * j + core == t)
-
-    for j in range(half):
-
-        def keep(b, j=j):
-            summed[j, block(b, many), :] = result(b, 2 * j + core).astype(BF16)
-
-        each(batches, keep)
-    for j in range(half):
-        pair(j).wait_recv()
-
-        def add(b, j=j):
-            rows = block(b, many)
-            summed[j, rows, :] = (summed[j, rows, :].astype(F32) + came[j, rows, :].astype(F32)).astype(BF16)
-
-        each(batches, add)
-
-        def send(d, j=j):
-            @pl.when(jnp.logical_not(same(j, d)))
-            def _():
-                back(j, d).start()
-
-        each(n_ep, send, order=None if far_first is None else far_first + [0])
-
-    landed[me] = summed[t // 2, own_rows, :]
-
-    def take(index):
-        @pl.when(index != me)
-        def _():
-            where = landed.at[index]
-            remote(where, where, back_send.at[0, 0], back_recv.at[index], (e, t)).wait_recv()
-
-    each(n_ep * half, take)
-    out_ref[...] = own_stream.astype(F32) + jnp.sum(landed[...].astype(F32), axis=0)
+            summed.at[final, block(there, seqs), :],
+            landed.at[d - 1],
+            back_send.at[d - 1],
+            back_recv.at[d - 1],
+            (there, t),
+        )
+
+    for j, mask in enumerate(masks):
+        if batches == 1:
+            whole = result(0, flip(t, mask))
+            pair(j).wait_recv()
+            summed[j] = (whole + came[j].astype(F32)).astype(BF16)
+        else:
+            pair(j).wait_recv()
+
+            def keep(b, j=j, mask=mask):
+                rows = block(b, many)
+                whole = result(b, flip(t, mask)) + came[j, rows, :].astype(F32)
+                summed[j, rows, :] = whole.astype(BF16)
+
+            each(batches, keep)
+        if mask:
+            each(
+                n_ep,
+                lambda d, j=j: cross(j, d).start(),
+                order=None if far_first is None else far_first + [0],
+            )
+
+    def gathered(d):
+        rows = block((e + d) % n_ep, seqs)
+        whole = summed[final, rows, :].astype(F32)
+        for j in range(final):
+            cross(j, d).wait_recv()
+            whole = whole + crossed[j, rows, :].astype(F32)
+        return rows, whole
+
+    def pass_on(i):
+        d = i + 1
+        rows, whole = gathered(d)
+        summed[final, rows, :] = whole.astype(BF16)
+        back(d).start()
+
+    each(n_ep - 1, pass_on, order=None if far_first is None else [d - 1 for d in far_first])
+    _, local = gathered(0)
+    each(n_ep - 1, lambda i: back(i + 1).wait_recv())
+    out_ref[...] = own_stream.astype(F32) + local + jnp.sum(landed[...].astype(F32), axis=0)
 
     for mask in range(1, n_tp):
         heads_copy(mask).wait_send()
@@ -520,13 +533,9 @@
     each(n_ep, sent)
     for j in range(half):
         pair(j).wait_send()
-
-        def gone(d, j=j):
-            @pl.when(jnp.logical_not(same(j, d)))
-            def _():
-                back(j, d).wait_send()
-
-        each(n_ep, gone)
+    for j in range(final):
+        each(n_ep, lambda d, j=j: cross(j, d).wait_send())
+    each(n_ep - 1, lambda i: back(i + 1).wait_send())
 
 
 def on_device(
@@ -567,7 +576,7 @@
     lanes = -(-n_ep * held // LANES) * LANES
     vmem = pl.BlockSpec(memory_space=pltpu.VMEM)
     smem = pl.BlockSpec(memory_space=pltpu.SMEM)
-    hbm = pl.BlockSpec(memory_space=pl.ANY)
+    hbm = pl.BlockSpec(memory_space=pltpu.HBM)
     dma = pltpu.SemaphoreType.DMA
     layer_out, fresh = pl.pallas_call(
         functools.partial(layer_kernel, n_ep, n_tp, split),
@@ -603,7 +612,8 @@
             pltpu.VMEM((half, rows, quarter), BF16),
             pltpu.VMEM((half, rows, quarter), BF16),
             pltpu.VMEM((half, rows, quarter), BF16),
-            pltpu.VMEM((n_ep * half, seqs, quarter), BF16),
+            pltpu.VMEM((max(half - 1, 1), rows, quarter), BF16),
+            pltpu.VMEM((n_ep - 1, seqs, quarter), BF16),
             dma((7,)),
             dma((Q_CHUNKS + 2,)),
             dma((seqs,)),
@@ -617,8 +627,10 @@
             dma((n_tp, n_ep)),
             dma((half,)),
             dma((half,)),
-            dma((half, n_ep)),
-            dma((n_ep * half,)),
+            dma((max(half - 1, 1), n_ep)),
+            dma((max(half - 1, 1), n_ep)),
+            dma((n_ep - 1,)),
+            dma((n_ep - 1,)),
         ],
         compiler_params=pltpu.CompilerParams(
             collective_id=0, has_side_effects=True, vmem_limit_bytes=60 * 1024 * 1024

time: 46 us -> 46.6 us (1.013)
  Pallas kernels: 42.4 us -> 43 us
    pallas_call x1, Pallas kernels: 42.4 us -> 43 us  [on_device(): pl.pallas_call(functools.partial(layer_kernel, n_ep, n_tp, split), out_sh...]
where the time goes in v3:
time: 46.6 us; the launch traced here: 46.4 us
  Pallas kernels  43 us (92%)
  other arithmetic  2.68 us (6%)
  between operations  0.65 us (1%)
    pallas_call x1, Pallas kernels, on_device(): pl.pallas_call(functools.partial(layer_kernel, n_ep, n_tp, split), out_sh...  43 us
    convert_element_type x1, other arithmetic, on_device(): return (layer_out.astype(BF16), new_rows)  1.37 us
    reshape x1, other arithmetic, on_device(): new_rows = fresh.astype(BF16).reshape(seqs, groups, kv_cache.shape[3])  1.32 us

profile of v3, /device:TPU:0, one launch (start us, length us, event | category | flops | bytes accessed | tf_op | source)
XLA Modules:
  0.0 46.4 jit_solution(5752121819314899682)
XLA Ops:
  0.6 43.0 %shard_map.203 = (f32[16,512]{1,0:T(8,128)}, f32[16,256]{1,0:T(8,128)}) custom-call(s32[16]{0:T(128)} %lengths_ref.1, f32[4]{0:T(128)} %lam_ref.1, bf16[16,2048]{1,0:T(8,128)(2,1)} %resid_ref.1, f32[1,2048]{1,0:T(1,128)} %bitcast.8, f32[1,128]{1,0:T(1,128)} %bitcast.13, f32[1,2048]{1,0:T(1,128)} %bitcast.9, f32[1,2048]{1,0:T(1,128)} %bitcast.10, ...), custom_call_target="tpu_custom_call" | custom-call | tf_op jit(solution)/shard_map/pallas_call | solution.py:581
  43.7 1.4 %convert_element_type.6 = bf16[16,512]{1,0:T(8,128)(2,1)} convert(f32[16,512]{1,0:T(8,128)} %get-tuple-element.4) | non-fusion elementwise | flops 8192 | bytes 49152 | tf_op jit(solution)/shard_map/convert_element_type | solution.py:661
  45.0 1.3 %convert_bitcast_fusion = bf16[16,1,256]{2,0,1:T(8,128)(2,1)} fusion(f32[16,256]{1,0:T(8,128)} %get-tuple-element.5), kind=kLoop, calls=%fused_computation | loop fusion | flops 4096 | bytes 24576 | tf_op jit(solution)/shard_map/reshape | solution.py:660
